TPU v7x, 32 devices: a whole 2x2x4 slice. The times are simulated.
32 devices in a mesh: sp: 4 (over y, x), dp: 8 (over z, core).
Axes of the slice: x: 2, y: 2, z: 4, core: 2. Of those that a mesh axis runs over, the one named last changes fastest.
Arguments:
- tokens: bfloat16 [8, 1024, 2048], P('dp', 'sp'), may hold values from -200 to 200
- w_qdown: bfloat16 [2048, 512], P('dp'), may hold values from -0.125 to 0.125
- w_kvdown: bfloat16 [2048, 512], P('dp'), may hold values from -0.125 to 0.125
- w_rotary: bfloat16 [2048, 64], replicated, may hold values from -0.125 to 0.125
- q_gain: float32 [512], replicated, may hold values from 0.1 to 1.9
- kv_gain: float32 [512], replicated, may hold values from 0.1 to 1.9
- w_qup: bfloat16 [512, 3072], P('dp'), may hold values from -1 to 1
- w_kvup: bfloat16 [512, 4096], P('dp'), may hold values from -1 to 1
- w_out: bfloat16 [2048, 2048], P(None, 'dp'), may hold values from -0.125 to 0.125
- out_gain: float32 [2048], replicated, may hold values from 0.1 to 1.9
Outputs:
- mixed: bfloat16 [8, 1024, 2048], P('dp', 'sp')
All inputs are finite; a program needn't handle non-finite values.
Results may differ from a plain program's by a relative error of at most 0.01.
The roundings to bfloat16 on the way count: a program that leaves them out, or rounds other values in their place, can miss the bound.
Values may be sent and summed in bfloat16 or wider, within the bound.
A program may use at most 128 MiB of HBM per device.

v0:
```python
import math
import jax
import jax.numpy as jnp
from jax import lax
from jax.sharding import PartitionSpec as P

HEADS = 16
NOPE = 128
ROPE = 64
VDIM = 128
EPSILON = 1e-06
THETA = 10000.0


def norm_rows(values, gain):
    scale = lax.rsqrt(jnp.mean(values * values, axis=-1, keepdims=True) + EPSILON)
    return values * scale * gain


def rotate(values, cosine, sine):
    half = values.shape[-1] // 2
    first = values[..., :half]
    second = values[..., half:]
    return jnp.concatenate(
        [first * cosine - second * sine, second * cosine + first * sine], axis=-1
    )


def turn_tables(offset, count):
    positions = (offset + jnp.arange(count)).astype(jnp.float32)
    freqs = THETA ** (-jnp.arange(0, ROPE, 2).astype(jnp.float32) / ROPE)
    angles = positions[:, None] * freqs[None, :]
    return (jnp.cos(angles), jnp.sin(angles))


def make_queries(q_full, cosine, sine, heads_here):
    rows = q_full.shape[0]
    shaped = q_full.reshape(rows, heads_here, NOPE + ROPE)
    turned = rotate(shaped[..., NOPE:], cosine[:, None, :], sine[:, None, :])
    joined = jnp.concatenate([shaped[..., :NOPE], turned], axis=-1)
    return joined.reshape(rows, heads_here * (NOPE + ROPE)).astype(jnp.bfloat16)


def attend(query_heads, keyval_heads, key_rot, heads_here):
    length = query_heads.shape[0]
    block = math.gcd(length, 512)
    scaling = (NOPE + ROPE) ** (-0.5)
    queries = query_heads.reshape(length, heads_here, NOPE + ROPE)
    keyval = keyval_heads.reshape(length, heads_here, NOPE + VDIM)
    keys_all = keyval[..., :NOPE]
    values_all = keyval[..., NOPE:]
    outputs = []
    for begin in range(0, length, block):
        finish = begin + block
        query_block = queries[begin:finish]
        scores = jnp.einsum(
            "qhd,khd->hqk",
            query_block[..., :NOPE],
            keys_all[:finish],
            preferred_element_type=jnp.float32,
        )
        scores = scores + jnp.einsum(
            "qhd,kd->hqk",
            query_block[..., NOPE:],
            key_rot[:finish],
            preferred_element_type=jnp.float32,
        )
        scores = scores * scaling
        query_pos = begin + jnp.arange(block)
        key_pos = jnp.arange(finish)
        allowed = key_pos[None, :] <= query_pos[:, None]
        scores = jnp.where(allowed[None], scores, -jnp.inf)
        top = jnp.max(scores, axis=-1, keepdims=True)
        expo = jnp.exp(scores - top)
        weights = (expo / jnp.sum(expo, axis=-1, keepdims=True)).astype(jnp.bfloat16)
        attended = jnp.einsum(
            "hqk,khd->qhd", weights, values_all[:finish], preferred_element_type=jnp.float32
        )
        outputs.append(attended.astype(jnp.bfloat16))
    return jnp.concatenate(outputs, axis=0).reshape(length, heads_here * VDIM)


def body(tokens, w_qdown, w_kvdown, w_rotary, q_gain, kv_gain, w_qup, w_kvup, w_out, out_gain):
    own_rows = tokens[0]
    tok_count = own_rows.shape[0]
    sp_count = lax.axis_size("sp")
    sp_place = lax.axis_index("sp")
    length = tok_count * sp_count
    heads_here = HEADS // sp_count
    pieces = (
        lax.all_gather(w_qdown, "dp", axis=0, tiled=True),
        lax.all_gather(w_kvdown, "dp", axis=0, tiled=True),
    )
    q_lat = jnp.dot(own_rows, pieces[0], preferred_element_type=jnp.float32)
    kv_lat = jnp.dot(own_rows, pieces[1], preferred_element_type=jnp.float32)
    q_norm = norm_rows(q_lat, q_gain).astype(jnp.bfloat16)
    kv_norm = norm_rows(kv_lat, kv_gain).astype(jnp.bfloat16)
    own_cos, own_sin = turn_tables(sp_place * tok_count, tok_count)
    key_rot = rotate(
        jnp.dot(own_rows, w_rotary, preferred_element_type=jnp.float32), own_cos, own_sin
    ).astype(jnp.bfloat16)
    q_all, kv_all, rot_all = (
        lax.all_gather(q_norm, "sp", axis=0, tiled=True),
        lax.all_gather(kv_norm, "sp", axis=0, tiled=True),
        lax.all_gather(key_rot, "sp", axis=0, tiled=True),
    )
    q_width = heads_here * (NOPE + ROPE)
    kv_width = heads_here * (NOPE + VDIM)
    q_columns = lax.dynamic_slice_in_dim(w_qup, sp_place * q_width, q_width, 1)
    kv_columns = lax.dynamic_slice_in_dim(w_kvup, sp_place * kv_width, kv_width, 1)
    pieces = (
        lax.all_gather(q_columns, "dp", axis=0, tiled=True),
        lax.all_gather(kv_columns, "dp", axis=0, tiled=True),
    )
    q_full = jnp.dot(q_all, pieces[0], preferred_element_type=jnp.float32)
    kv_full = jnp.dot(kv_all, pieces[1], preferred_element_type=jnp.float32)
    all_cos, all_sin = turn_tables(0, length)
    query_heads = make_queries(q_full, all_cos, all_sin, heads_here)
    keyval_heads = kv_full.astype(jnp.bfloat16)
    attended = attend(query_heads, keyval_heads, rot_all, heads_here)
    merged = lax.all_to_all(attended, "sp", split_axis=0, concat_axis=1, tiled=True)
    proj = jnp.dot(
        merged, lax.all_gather(w_out, "dp", axis=1, tiled=True), preferred_element_type=jnp.float32
    )
    mixed = norm_rows(proj, out_gain).astype(jnp.bfloat16)
    return mixed[None]


def solution(mesh):
    in_specs = (
        P("dp", "sp", None),
        P("dp", None),
        P("dp", None),
        P(),
        P(),
        P(),
        P("dp", None),
        P("dp", None),
        P(None, "dp"),
        P(),
    )
    out_specs = P("dp", "sp", None)
    return jax.shard_map(body, mesh=mesh, in_specs=in_specs, out_specs=out_specs, check_vma=False)
```

profile of v0, /device:TPU:0, one launch (start us, length us, event | category | flops | bytes accessed | tf_op | source)
XLA Modules:
  0.0 248.7 jit_solution(12525613199316772031)
XLA Ops:
  8.1 32.8 %all-gather.13.cloned.1.call-done = bf16[2048,512]{1,0:T(8,128)(2,1)} async-done(((bf16[256,512]{1,0:T(8,128)(2,1)}), bf16[2048,512]{1,0:T(8,128)(2,1)}) %all-gather.13.cloned.1.call-update) | async-done | bytes 2097168 | tf_op jit(solution)/shard_map/all_gather | solution.py:91
  40.8 2.4 multiply_reduce_fusion.1
  43.3 0.9 multiply_convert_fusion.1
  44.2 1.6 constant_dynamic-slice_fusion.1
  45.8 25.2 %all-gather.7.cloned.1.call-done = bf16[2048,512]{1,0:T(8,128)(2,1)} async-done(((bf16[256,512]{1,0:T(8,128)(2,1)}), bf16[2048,512]{1,0:T(8,128)(2,1)}) %all-gather.7.cloned.1.call-update) | async-done | bytes 2097168 | tf_op jit(solution)/shard_map/all_gather | solution.py:92
  71.0 2.4 multiply_reduce_fusion.2
  73.4 0.8 multiply_convert_fusion.2
  75.5 10.3 %all_gather.30 = bf16[1024,64]{0,1:T(8,128)(2,1)S(1)} all-gather(bf16[256,64]{0,1:T(8,128)(2,1)S(1)} %pad_maximum_fusion.3), channel_id=1, replica_groups=mesh['sp'=4,'dp'=8] {'sp'}, dimensions={0}, use_global_device_ids=true | all-gather | bytes 163840 | tf_op jit(solution)/shard_map/all_gather | solution.py:105
  85.9 0.9 constant_dynamic-slice_fusion
  87.6 1.3 multiply_cosine_fusion
  88.8 1.2 iota_compare_fusion
  90.0 15.7 %all_gather.29 = bf16[512,768]{1,0:T(8,128)(2,1)S(1)} all-gather(bf16[64,768]{1,0:T(8,128)(2,1)S(1)} %constant_dynamic-slice_fusion), channel_id=1, replica_groups=mesh['sp'=4,'dp'=8] {'dp'}, dimensions={0}, use_global_device_ids=true | all-gather | bytes 884736 | tf_op jit(solution)/shard_map/all_gather | solution.py:112
  105.7 4.0 %fusion.45 = f32[1024,768]{0,1:T(8,128)} fusion(bf16[1024,512]{1,0:T(8,128)(2,1)} %all-gather.15.cloned.1.call-done, bf16[512,768]{1,0:T(8,128)(2,1)S(1)} %all_gather.29), kind=kOutput, calls=%fused_computation.80 | convolution fusion | flops 805306368 | bytes 4980736 | tf_op jit(solution)/shard_map/dot_general | solution.py:115
  109.7 3.3 %copy.16 = bf16[1024,4,192]{2,0,1:T(8,128)(2,1)S(1)} copy(f32[1024,4,192]{0,2,1:T(8,128)} %bitcast.55) | data formatting | bytes 4718592 | tf_op jit(solution)/shard_map/reshape | solution.py:38
  112.9 2.1 subtract_convert_fusion
  115.1 7.9 %all-gather.11.cloned.1.call-done = bf16[512,1024]{1,0:T(8,128)(2,1)} async-done(((bf16[64,1024]{1,0:T(8,128)(2,1)}), bf16[512,1024]{1,0:T(8,128)(2,1)}) %all-gather.11.cloned.1.call-update) | async-done | bytes 1048592 | tf_op jit(solution)/shard_map/all_gather | solution.py:113
  123.0 27.8 %all-gather.9.cloned.1.call-done = bf16[1024,512]{1,0:T(8,128)(2,1)} async-done(((bf16[256,512]{1,0:T(8,128)(2,1)}), bf16[1024,512]{1,0:T(8,128)(2,1)}) %all-gather.9.cloned.1.call-update) | async-done | bytes 1048592 | tf_op jit(solution)/shard_map/all_gather | solution.py:104
  150.8 2.8 %convolution_convert_fusion = bf16[1024,1024]{0,1:T(8,128)(2,1)S(1)} fusion(bf16[1024,512]{1,0:T(8,128)(2,1)} %all-gather.9.cloned.1.call-done, bf16[512,1024]{1,0:T(8,128)(2,1)} %all-gather.11.cloned.1.call-done), kind=kOutput, calls=%fused_computation.17 | convolution fusion | flops 1074790400 | bytes 4194304 | tf_op jit(solution)/shard_map/dot_general | solution.py:116
  155.1 1.0 fusion.5
  156.1 2.0 copy-done.2
  158.0 0.8 fusion.44
  158.8 6.5 %fusion.11 = bf16[512,4,128]{0,2,1:T(8,128)(2,1)} fusion(f32[4,512]{1,0:T(4,128)S(1)} %fusion.44, bf16[1024,4,256]{0,2,1:T(8,128)(2,1)} %bitcast.59, f32[4,512,512]{1,2,0:T(8,128)} %copy-done.2), kind=kOutput, calls=%fused_computation.21 | convolution fusion | flops 271845888 | bytes 9445376 | tf_op jit(solution)/shard_map/hqk,khd->qhd/dot_general | solution.py:76
  165.4 2.4 fusion.28
  167.7 1.8 fusion.3
  169.6 3.2 %copy-done.1 = f32[4,512,1024]{2,1,0:T(8,128)} copy-done((f32[4,512,1024]{2,1,0:T(8,128)}, f32[4,512,1024]{2,1,0:T(8,128)S(1)}, u32[]{:S(2)}) %copy-start.1) | copy-done | bytes 8388632
  172.8 2.0 fusion.43
  174.9 11.1 %fusion.10 = bf16[512,4,128]{0,2,1:T(8,128)(2,1)} fusion(f32[4,512]{1,0:T(4,128)S(1)} %fusion.43, bf16[1024,4,256]{0,2,1:T(8,128)(2,1)S(1)} %bitcast.61, f32[4,512,1024]{2,1,0:T(8,128)} %copy-done.1), kind=kOutput, calls=%fused_computation.20 | convolution fusion | flops 543427584 | bytes 18358272 | tf_op jit(solution)/shard_map/hqk,khd->qhd/dot_general | solution.py:76
  186.0 1.3 pad_maximum_fusion
  188.3 16.8 %all_to_all.19 = bf16[4,256,512]{1,2,0:T(8,128)(2,1)S(1)} all-to-all(bf16[4,256,512]{1,2,0:T(8,128)(2,1)S(1)} %copy.21), channel_id=1, replica_groups=mesh['sp'=4,'dp'=8] {'sp'}, dimensions={0} | all-to-all | bytes 2097152 | tf_op jit(solution)/shard_map/all_to_all | solution.py:121
  205.1 29.7 %all-gather.17.cloned.1.call-done = bf16[2048,2048]{1,0:T(8,128)(2,1)} async-done(((bf16[2048,256]{1,0:T(8,128)(2,1)}), bf16[2048,2048]{1,0:T(8,128)(2,1)}) %all-gather.17.cloned.1.call-update) | async-done | bytes 8388624 | tf_op jit(solution)/shard_map/all_gather | solution.py:123
  234.8 5.8 %multiply_reduce_fusion = (f32[256]{0:T(256)S(1)}, f32[256,2048]{1,0:T(8,128)S(1)}) fusion(bf16[256,2048]{0,1:T(8,128)(2,1)S(1)} %bitcast.57, bf16[2048,2048]{1,0:T(8,128)(2,1)} %all-gather.17.cloned.1.call-done), kind=kOutput, calls=%fused_computation.14 | convolution fusion | flops 2148531968 | bytes 11535360 | tf_op jit(solution)/shard_map/dot_general | solution.py:122
  240.6 1.2 fusion.12
  (51 shorter events, 6.0 us)
Async XLA Ops:
  6.5 34.3 %copy-start = (bf16[1,256,2048]{2,1,0:T(8,128)(2,1)S(1)}, bf16[1,256,2048]{2,1,0:T(8,128)(2,1)}, u32[]{:S(2)}) copy-start(bf16[1,256,2048]{2,1,0:T(8,128)(2,1)} %param.10) | copy-start | bytes 3145732
  6.5 36.7 %copy-start.11 = (f32[512]{0:T(512)S(1)}, f32[512]{0:T(512)}, u32[]{:S(2)}) copy-start(f32[512]{0:T(512)} %param.14) | copy-start | bytes 6148
  6.5 34.3 %all-gather.13.cloned.1.call-start = ((), (), s32[]{:S(2)}) async-start(), calls=%async_computation.4 | async-start | bytes 2359296 | tf_op jit(solution)/shard_map/all_gather | solution.py:91
  7.3 63.8 %all-gather.7.cloned.1.call-start = ((), (), s32[]{:S(2)}) async-start(), calls=%async_computation.1 | async-start | bytes 2359296 | tf_op jit(solution)/shard_map/all_gather | solution.py:92
  8.0 65.4 %copy-start.12 = (f32[512]{0:T(512)S(1)}, f32[512]{0:T(512)}, u32[]{:S(2)}) copy-start(f32[512]{0:T(512)} %param.15) | copy-start | bytes 6148
  8.0 97.7 %all-gather.15.cloned.1.call-start = ((), (), s32[]{:S(2)}) async-start(), calls=%async_computation.5 | async-start | bytes 1310720 | tf_op jit(solution)/shard_map/all_gather | solution.py:103
  43.2 31.7 %copy-start.9 = (bf16[2048,64]{0,1:T(8,128)(2,1)S(1)}, bf16[2048,64]{0,1:T(8,128)(2,1)}, u32[]{:S(2)}) copy-start(bf16[2048,64]{0,1:T(8,128)(2,1)} %param.13) | copy-start | bytes 786436
  44.1 78.9 %all-gather.11.cloned.1.call-start = ((), (), s32[]{:S(2)}) async-start(), calls=%async_computation.3 | async-start | bytes 1179648 | tf_op jit(solution)/shard_map/all_gather | solution.py:113
  45.8 105.0 %all-gather.9.cloned.1.call-start = ((), (), s32[]{:S(2)}) async-start(), calls=%async_computation.2 | async-start | bytes 1310720 | tf_op jit(solution)/shard_map/all_gather | solution.py:104
  74.3 160.5 %all-gather.17.cloned.1.call-start = ((), (), s32[]{:S(2)}) async-start(), calls=%async_computation.6 | async-start | bytes 9437184 | tf_op jit(solution)/shard_map/all_gather | solution.py:123
  153.7 1.3 copy-start.5
  153.7 1.3 copy-start.3
  153.7 1.4 copy-start.8
  156.1 2.0 copy-start.2
  165.4 2.4 copy-start.4
  165.4 2.4 copy-start.6
  169.6 3.2 %copy-start.1 = (f32[4,512,1024]{2,1,0:T(8,128)}, f32[4,512,1024]{2,1,0:T(8,128)S(1)}, u32[]{:S(2)}) copy-start(f32[4,512,1024]{2,1,0:T(8,128)S(1)} %fusion.3) | copy-start | bytes 25165828
  172.8 2.0 copy-start.7
  234.8 5.8 %copy-start.10 = (f32[2048]{0:T(1024)S(1)}, f32[2048]{0:T(1024)}, u32[]{:S(2)}) copy-start(f32[2048]{0:T(1024)} %param.19) | copy-start | bytes 24580
Sparse Core Ops, SparseCore 0:
  8.9 31.8 all-gather.12
  42.4 28.5 all-gather.6
  72.9 26.3 all-gather.14
  100.8 22.2 all-gather.10
  124.7 26.0 all-gather.8
  152.3 82.4 all-gather.16
where the time goes:
time: 249 us
  waiting for transfers between devices  125 us (50%)
  blocking collectives  42.8 us (17%)
  matrix products  41.4 us (17%)
  between operations  13.7 us (6%)
  other arithmetic  12.7 us (5%)
  local copies, waits for them, and re-layouts  12.5 us (5%)
    all_gather x1, waiting for transfers between devices, body(): lax.all_gather(w_qdown, 'dp', axis=0, tiled=True)  32.8 us
    all_gather x1, waiting for transfers between devices, body(): lax.all_gather(w_out, 'dp', axis=1, tiled=True)  29.7 us
    all_gather x1, waiting for transfers between devices, body(): lax.all_gather(kv_norm, 'sp', axis=0, tiled=True)  27.8 us
    all_gather x1, waiting for transfers between devices, body(): lax.all_gather(w_kvdown, 'dp', axis=0, tiled=True)  25.2 us
    dot_general x2, matrix products, attend(): jnp.einsum('hqk,khd->qhd', weights, values_all[:finish], preferred_elemen...  17.6 us
    all_to_all x1, blocking collectives, body(): lax.all_to_all(attended, 'sp', split_axis=0, concat_axis=1, tiled=True)  16.8 us
    all_gather x1, blocking collectives, body(): lax.all_gather(q_columns, 'dp', axis=0, tiled=True)  15.7 us
    all_gather x1, blocking collectives, body(): lax.all_gather(key_rot, 'sp', axis=0, tiled=True)  10.3 us
  transfers between devices with their start and end apart: 6, of which 5 were waited for; matrix products, arithmetic and copies ran while one was open for 21% of the time, Pallas kernels for 0%

commit v1 on v0

--- a/solution.py
+++ b/solution.py
@@ -1,3 +1,4 @@
+import functools
 import math
 import jax
 import jax.numpy as jnp
@@ -10,6 +11,28 @@
 VDIM = 128
 EPSILON = 1e-06
 THETA = 10000.0
+
+
+def proceed_the_array(z_in, where_dim):
+    z_in = jnp.moveaxis(z_in, 0, where_dim)
+    e_next = z_in.shape
+    return z_in.reshape(
+        *e_next[:where_dim], e_next[where_dim] * e_next[where_dim + 1], *e_next[where_dim + 2 :]
+    )
+
+
+def apply_the_records(state, mesh_ax, along_dim):
+    n_slots = jax.lax.axis_size(mesh_ax)
+    pages = list(map(lambda dev_i: (dev_i, (dev_i + 1) % n_slots), range(n_slots)))
+    heap = [state]
+    while len(heap) < n_slots:
+        heap.append(jax.lax.ppermute(heap[-1], axis_name=mesh_ax, perm=pages))
+    x_now = jax.lax.axis_index(mesh_ax)
+    heap = jnp.stack(heap, axis=0)[(x_now - jnp.arange(n_slots)) % n_slots]
+    return proceed_the_array(heap, along_dim)
+
+
+write_the_levels_all = functools.partial(apply_the_records, mesh_ax="sp", along_dim=0)
 
 
 def norm_rows(values, gain):
@@ -101,7 +124,7 @@
     ).astype(jnp.bfloat16)
     q_all, kv_all, rot_all = (
         lax.all_gather(q_norm, "sp", axis=0, tiled=True),
-        lax.all_gather(kv_norm, "sp", axis=0, tiled=True),
+        write_the_levels_all(kv_norm),
         lax.all_gather(key_rot, "sp", axis=0, tiled=True),
     )
     q_width = heads_here * (NOPE + ROPE)

time: 249 us -> 225 us (0.904)
  waiting for transfers between devices: 125 us -> 95.6 us
  blocking collectives: 42.8 us -> 45.9 us
    all_gather x1 -> x0, waiting for transfers between devices: 27.8 us -> none  [body(): lax.all_gather(kv_norm, 'sp', axis=0, tiled=True)]
    all_gather x1, waiting for transfers between devices: 25.2 us -> 9.78 us  [body(): lax.all_gather(w_kvdown, 'dp', axis=0, tiled=True)]
    all_gather x1, waiting for transfers between devices: 0.01 us -> 14.7 us  [body(): lax.all_gather(q_norm, 'sp', axis=0, tiled=True)]
    ppermute x0 -> x3, waiting for transfers between devices: none -> 13.4 us  [apply_the_records(): heap.append(jax.lax.ppermute(heap[-1], axis_name=mesh_ax, perm=pages))]
    all_gather x1, waiting for transfers between devices: 7.94 us -> 0.01 us  [body(): lax.all_gather(kv_columns, 'dp', axis=0, tiled=True)]
    all_gather x1, waiting for transfers between devices: 29.7 us -> 24.6 us  [body(): lax.all_gather(w_out, 'dp', axis=1, tiled=True)]
    all_gather x1, blocking collectives: 15.7 us -> 18.9 us  [body(): lax.all_gather(q_columns, 'dp', axis=0, tiled=True)]
    unnamed x26 -> x24, local copies, waits for them, and re-layouts: 5.87 us -> 5.23 us
  transfers between devices with their start and end apart: 6 -> 8, of which waited for: 5 -> 6; matrix products, arithmetic and copies ran while one was open for 21% -> 24% of each run, Pallas kernels for 0% -> 0%
where the time goes in v1:
time: 225 us
  waiting for transfers between devices  95.6 us (42%)
  blocking collectives  45.9 us (20%)
  matrix products  42.6 us (19%)
  local copies, waits for them, and re-layouts  13.5 us (6%)
  between operations  13.4 us (6%)
  other arithmetic  11.6 us (5%)
  starting transfers between devices  2.25 us (1%)
    all_gather x1, waiting for transfers between devices, body(): lax.all_gather(w_qdown, 'dp', axis=0, tiled=True)  31.1 us
    all_gather x1, waiting for transfers between devices, body(): lax.all_gather(w_out, 'dp', axis=1, tiled=True)  24.6 us
    all_gather x1, blocking collectives, body(): lax.all_gather(q_columns, 'dp', axis=0, tiled=True)  18.9 us
    all_to_all x1, blocking collectives, body(): lax.all_to_all(attended, 'sp', split_axis=0, concat_axis=1, tiled=True)  16.6 us
    dot_general x2, matrix products, attend(): jnp.einsum('hqk,khd->qhd', weights, values_all[:finish], preferred_elemen...  16.3 us
    all_gather x1, waiting for transfers between devices, body(): lax.all_gather(q_norm, 'sp', axis=0, tiled=True)  14.7 us
    ppermute x3, waiting for transfers between devices, apply_the_records(): heap.append(jax.lax.ppermute(heap[-1], axis_name=mesh_ax, perm=pages))  13.4 us
    all_gather x1, blocking collectives, body(): lax.all_gather(key_rot, 'sp', axis=0, tiled=True)  10.4 us
  transfers between devices with their start and end apart: 8, of which 6 were waited for; matrix products, arithmetic and copies ran while one was open for 24% of the time, Pallas kernels for 0%

profile of v1, /device:TPU:0, one launch (start us, length us, event | category | flops | bytes accessed | tf_op | source)
XLA Modules:
  0.0 224.9 jit_solution(14636101389494083188)
XLA Ops:
  8.1 1.6 constant_dynamic-slice_fusion.1
  9.7 31.1 %all-gather.10.cloned.1.call-done = bf16[2048,512]{1,0:T(8,128)(2,1)} async-done(((bf16[256,512]{1,0:T(8,128)(2,1)}), bf16[2048,512]{1,0:T(8,128)(2,1)}) %all-gather.10.cloned.1.call-update) | async-done | bytes 2097168 | tf_op jit(solution)/shard_map/all_gather | solution.py:114
  40.8 2.4 %multiply_reduce_fusion.1 = (f32[256]{0:T(256)S(1)}, f32[256,512]{1,0:T(8,128)S(1)}) fusion(bf16[2048,512]{1,0:T(8,128)(2,1)} %all-gather.10.cloned.1.call-done, bf16[1,256,2048]{2,1,0:T(8,128)(2,1)S(1)} %copy-done), kind=kOutput, calls=%fused_computation.45 | convolution fusion | flops 537132800 | bytes 3671040 | tf_op jit(solution)/shard_map/dot_general | solution.py:117
  47.1 18.9 %all_gather.25 = bf16[512,768]{1,0:T(8,128)(2,1)S(1)} all-gather(bf16[64,768]{1,0:T(8,128)(2,1)S(1)} %constant_dynamic-slice_fusion), channel_id=1, replica_groups=mesh['sp'=4,'dp'=8] {'dp'}, dimensions={0}, use_global_device_ids=true | all-gather | bytes 884736 | tf_op jit(solution)/shard_map/all_gather | solution.py:135
  66.1 9.8 %all-gather.6.cloned.1.call-done = bf16[2048,512]{1,0:T(8,128)(2,1)} async-done(((bf16[256,512]{1,0:T(8,128)(2,1)}), bf16[2048,512]{1,0:T(8,128)(2,1)}) %all-gather.6.cloned.1.call-update) | async-done | bytes 2097168 | tf_op jit(solution)/shard_map/all_gather | solution.py:115
  75.8 2.4 %multiply_reduce_fusion.2 = (f32[256]{0:T(256)S(1)}, f32[256,512]{1,0:T(8,128)S(1)}) fusion(bf16[2048,512]{1,0:T(8,128)(2,1)} %all-gather.6.cloned.1.call-done, bf16[1,256,2048]{2,1,0:T(8,128)(2,1)S(1)} %copy-done), kind=kOutput, calls=%fused_computation.47 | convolution fusion | flops 537132800 | bytes 3671040 | tf_op jit(solution)/shard_map/dot_general | solution.py:118
  78.4 1.5 collective-permute-start
  79.9 1.2 multiply_cosine_fusion
  81.1 6.6 %collective-permute-done = bf16[256,512]{1,0:T(8,128)(2,1)S(1)} collective-permute-done((bf16[256,512]{1,0:T(8,128)(2,1)S(1)}, bf16[256,512]{1,0:T(8,128)(2,1)S(1)}, u32[]{:S(2)}, u32[]{:S(2)}) %collective-permute-start) | collective-permute-done | bytes 262176 | tf_op jit(solution)/shard_map/ppermute | solution.py:29
  88.3 1.2 iota_compare_fusion
  89.5 6.7 %collective-permute-done.1 = bf16[256,512]{1,0:T(8,128)(2,1)S(1)} collective-permute-done((bf16[256,512]{1,0:T(8,128)(2,1)S(1)}, bf16[256,512]{1,0:T(8,128)(2,1)S(1)}, u32[]{:S(2)}, u32[]{:S(2)}) %collective-permute-start.1) | collective-permute-done | bytes 262176 | tf_op jit(solution)/shard_map/ppermute | solution.py:29
  96.2 10.4 %all_gather.26 = bf16[1024,64]{0,1:T(8,128)(2,1)S(1)} all-gather(bf16[256,64]{0,1:T(8,128)(2,1)S(1)} %pad_maximum_fusion.4), channel_id=1, replica_groups=mesh['sp'=4,'dp'=8] {'sp'}, dimensions={0}, use_global_device_ids=true | all-gather | bytes 163840 | tf_op jit(solution)/shard_map/all_gather | solution.py:128
  106.9 1.6 gather_fusion
  108.5 4.2 %convolution_convert_fusion = bf16[1024,1024]{0,1:T(8,128)(2,1)} fusion(bf16[1024,512]{1,0:T(8,128)(2,1)} %bitcast.70, bf16[512,1024]{1,0:T(8,128)(2,1)} %all-gather.8.cloned.1.call-done), kind=kOutput, calls=%fused_computation.18 | convolution fusion | flops 1074790400 | bytes 4194304 | tf_op jit(solution)/shard_map/dot_general | solution.py:139
  112.7 14.7 %all-gather.12.cloned.1.call-done = bf16[1024,512]{1,0:T(8,128)(2,1)} async-done(((bf16[256,512]{1,0:T(8,128)(2,1)}), bf16[1024,512]{1,0:T(8,128)(2,1)}) %all-gather.12.cloned.1.call-update) | async-done | bytes 1048592 | tf_op jit(solution)/shard_map/all_gather | solution.py:126
  127.4 4.0 %fusion.47 = f32[1024,768]{0,1:T(8,128)} fusion(bf16[1024,512]{1,0:T(8,128)(2,1)} %all-gather.12.cloned.1.call-done, bf16[512,768]{1,0:T(8,128)(2,1)S(1)} %all_gather.25), kind=kOutput, calls=%fused_computation.89 | convolution fusion | flops 805306368 | bytes 4980736 | tf_op jit(solution)/shard_map/dot_general | solution.py:138
  131.4 3.1 %copy.16 = bf16[1024,4,192]{2,0,1:T(8,128)(2,1)S(1)} copy(f32[1024,4,192]{0,2,1:T(8,128)} %bitcast.63) | data formatting | bytes 4718592 | tf_op jit(solution)/shard_map/reshape | solution.py:61
  134.5 1.6 subtract_convert_fusion
  136.1 2.0 fusion.22
  139.0 2.0 copy-done.2
  141.8 5.7 %fusion.11 = bf16[512,4,128]{0,2,1:T(8,128)(2,1)} fusion(f32[4,512]{1,0:T(4,128)S(1)} %fusion.46, bf16[1024,4,256]{0,2,1:T(8,128)(2,1)} %bitcast.67, f32[4,512,512]{1,2,0:T(8,128)} %copy-done.2), kind=kOutput, calls=%fused_computation.22 | convolution fusion | flops 271845888 | bytes 9445376 | tf_op jit(solution)/shard_map/hqk,khd->qhd/dot_general | solution.py:99
  147.5 2.3 %fusion.28 = f32[1024,512,4]{0,1,2:T(8,128)S(1)} fusion(bf16[1024,4,32]{0,2,1:T(8,128)(2,1)} %copy-done.3, bf16[1024,4,32]{0,2,1:T(8,128)(2,1)S(1)} %get-tuple-element.5, bf16[1024,64]{0,1:T(8,128)(2,1)S(1)} %all_gather.26), kind=kOutput, calls=%fused_computation.50 | convolution fusion | flops 268959744 | bytes 9043968 | tf_op jit(solution)/shard_map/qhd,kd->hqk/dot_general | solution.py:85
  149.8 1.8 fusion.3
  151.7 3.2 %copy-done.1 = f32[4,512,1024]{2,1,0:T(8,128)} copy-done((f32[4,512,1024]{2,1,0:T(8,128)}, f32[4,512,1024]{2,1,0:T(8,128)S(1)}, u32[]{:S(2)}) %copy-start.1) | copy-done | bytes 8388632
  154.9 2.0 fusion.45
  157.0 10.6 %fusion.10 = bf16[512,4,128]{0,2,1:T(8,128)(2,1)} fusion(f32[4,512]{1,0:T(4,128)S(1)} %fusion.45, bf16[1024,4,256]{0,2,1:T(8,128)(2,1)S(1)} %bitcast.69, f32[4,512,1024]{2,1,0:T(8,128)} %copy-done.1), kind=kOutput, calls=%fused_computation.21 | convolution fusion | flops 543427584 | bytes 18358272 | tf_op jit(solution)/shard_map/hqk,khd->qhd/dot_general | solution.py:99
  167.6 1.3 pad_maximum_fusion.1
  168.9 1.0 all_to_all.14
  170.1 16.6 %all_to_all.19 = bf16[4,256,512]{1,2,0:T(8,128)(2,1)S(1)} all-to-all(bf16[4,256,512]{1,2,0:T(8,128)(2,1)S(1)} %copy.21), channel_id=1, replica_groups=mesh['sp'=4,'dp'=8] {'sp'}, dimensions={0} | all-to-all | bytes 2097152 | tf_op jit(solution)/shard_map/all_to_all | solution.py:144
  186.7 24.6 %all-gather.14.cloned.1.call-done = bf16[2048,2048]{1,0:T(8,128)(2,1)} async-done(((bf16[2048,256]{1,0:T(8,128)(2,1)}), bf16[2048,2048]{1,0:T(8,128)(2,1)}) %all-gather.14.cloned.1.call-update) | async-done | bytes 8388624 | tf_op jit(solution)/shard_map/all_gather | solution.py:146
  211.3 5.8 %multiply_reduce_fusion = (f32[256]{0:T(256)S(1)}, f32[256,2048]{1,0:T(8,128)S(1)}) fusion(bf16[256,2048]{0,1:T(8,128)(2,1)S(1)} %bitcast.65, bf16[2048,2048]{1,0:T(8,128)(2,1)} %all-gather.14.cloned.1.call-done), kind=kOutput, calls=%fused_computation.15 | convolution fusion | flops 2148531968 | bytes 11535360 | tf_op jit(solution)/shard_map/dot_general | solution.py:145
  217.2 1.2 fusion.12
  (57 shorter events, 8.3 us)
Async XLA Ops:
  6.5 34.3 %copy-start = (bf16[1,256,2048]{2,1,0:T(8,128)(2,1)S(1)}, bf16[1,256,2048]{2,1,0:T(8,128)(2,1)}, u32[]{:S(2)}) copy-start(bf16[1,256,2048]{2,1,0:T(8,128)(2,1)} %param.10) | copy-start | bytes 3145732
  6.5 36.7 %copy-start.11 = (f32[512]{0:T(512)S(1)}, f32[512]{0:T(512)}, u32[]{:S(2)}) copy-start(f32[512]{0:T(512)} %param.14) | copy-start | bytes 6148
  6.5 38.2 %copy-start.8 = (bf16[2048,64]{0,1:T(8,128)(2,1)S(1)}, bf16[2048,64]{0,1:T(8,128)(2,1)}, u32[]{:S(2)}) copy-start(bf16[2048,64]{0,1:T(8,128)(2,1)} %param.13) | copy-start | bytes 786436
  6.5 34.3 %all-gather.10.cloned.1.call-start = ((), (), s32[]{:S(2)}) async-start(), calls=%async_computation.3 | async-start | bytes 2359296 | tf_op jit(solution)/shard_map/all_gather | solution.py:114
  7.3 68.6 %all-gather.6.cloned.1.call-start = ((), (), s32[]{:S(2)}) async-start(), calls=%async_computation.1 | async-start | bytes 2359296 | tf_op jit(solution)/shard_map/all_gather | solution.py:115
  8.0 100.5 %all-gather.8.cloned.1.call-start = ((), (), s32[]{:S(2)}) async-start(), calls=%async_computation.2 | async-start | bytes 1179648 | tf_op jit(solution)/shard_map/all_gather | solution.py:136
  9.7 117.7 %all-gather.12.cloned.1.call-start = ((), (), s32[]{:S(2)}) async-start(), calls=%async_computation.4 | async-start | bytes 1310720 | tf_op jit(solution)/shard_map/all_gather | solution.py:126
  44.1 34.2 %copy-start.10 = (f32[512]{0:T(512)S(1)}, f32[512]{0:T(512)}, u32[]{:S(2)}) copy-start(f32[512]{0:T(512)} %param.15) | copy-start | bytes 6148
  44.1 167.2 %all-gather.14.cloned.1.call-start = ((), (), s32[]{:S(2)}) async-start(), calls=%async_computation.5 | async-start | bytes 9437184 | tf_op jit(solution)/shard_map/all_gather | solution.py:146
  78.4 9.4 %collective-permute-start = (bf16[256,512]{1,0:T(8,128)(2,1)S(1)}, bf16[256,512]{1,0:T(8,128)(2,1)S(1)}, u32[]{:S(2)}, u32[]{:S(2)}) collective-permute-start(bf16[256,512]{1,0:T(8,128)(2,1)S(1)} %multiply_convert_fusion.2), channel_id=1, source_target_pairs={{0,8},{8,16},{16,24},{24,0},{1,9},{9,17},{17,25},{25,1},{2,10},{10... | collective-permute-start | bytes 786440 | tf_op jit(solution)/shard_map/ppermute | solution.py:29
  87.7 8.5 %collective-permute-start.1 = (bf16[256,512]{1,0:T(8,128)(2,1)S(1)}, bf16[256,512]{1,0:T(8,128)(2,1)S(1)}, u32[]{:S(2)}, u32[]{:S(2)}) collective-permute-start(bf16[256,512]{1,0:T(8,128)(2,1)S(1)} %collective-permute-done), channel_id=1, source_target_pairs={{0,8},{8,16},{16,24},{24,0},{1,9},{9,17},{17,25},{25,1},{2,10},{10... | collective-permute-start | bytes 786440 | tf_op jit(solution)/shard_map/ppermute | solution.py:29
  96.2 10.5 %collective-permute-start.2 = (bf16[256,512]{1,0:T(8,128)(2,1)S(1)}, bf16[256,512]{1,0:T(8,128)(2,1)S(1)}, u32[]{:S(2)}, u32[]{:S(2)}) collective-permute-start(bf16[256,512]{1,0:T(8,128)(2,1)S(1)} %collective-permute-done.1), channel_id=1, source_target_pairs={{0,8},{8,16},{16,24},{24,0},{1,9},{9,17},{17,25},{25,1},{2,10},{10... | collective-permute-start | bytes 786440 | tf_op jit(solution)/shard_map/ppermute | solution.py:29
  134.4 3.6 %copy-start.7 = (pred[512,512]{0,1:T(8,128)(4,1)S(1)}, pred[512,512]{0,1:T(8,128)(4,1)}, u32[]{:S(2)}) copy-start(pred[512,512]{0,1:T(8,128)(4,1)} %iota_compare_fusion.1) | copy-start | bytes 786436
  136.0 2.0 copy-start.3
  139.0 2.0 copy-start.2
  147.5 2.4 %copy-start.4 = (pred[512,1024]{1,0:T(8,128)(4,1)S(1)}, pred[512,1024]{1,0:T(8,128)(4,1)}, u32[]{:S(2)}) copy-start(pred[512,1024]{1,0:T(8,128)(4,1)} %iota_compare_fusion) | copy-start | bytes 1572868
  147.5 2.4 %copy-start.5 = (bf16[1024,1024]{0,1:T(8,128)(2,1)S(1)}, bf16[1024,1024]{0,1:T(8,128)(2,1)}, u32[]{:S(2)}) copy-start(bf16[1024,1024]{0,1:T(8,128)(2,1)} %convolution_convert_fusion) | copy-start | bytes 6291460
  151.7 3.2 %copy-start.1 = (f32[4,512,1024]{2,1,0:T(8,128)}, f32[4,512,1024]{2,1,0:T(8,128)S(1)}, u32[]{:S(2)}) copy-start(f32[4,512,1024]{2,1,0:T(8,128)S(1)} %fusion.3) | copy-start | bytes 25165828
  154.9 2.0 copy-start.6
  211.3 5.8 %copy-start.9 = (f32[2048]{0:T(1024)S(1)}, f32[2048]{0:T(1024)}, u32[]{:S(2)}) copy-start(f32[2048]{0:T(1024)} %param.19) | copy-start | bytes 24580
Sparse Core Ops, SparseCore 0:
  8.9 31.8 all-gather.9
  42.4 33.3 all-gather.5
  77.4 22.0 all-gather.7
  101.2 26.0 all-gather.11
  128.8 82.4 all-gather.13
